TPU v7x, 32 devices: a whole 2x2x4 slice. The times are simulated.
32 devices in a mesh: row: 8 (over z, core), col: 4 (over y, x).
Axes of the slice: x: 2, y: 2, z: 4, core: 2. Of those that a mesh axis runs over, the one named last changes fastest.
Arguments:
- tokens: bfloat16 [4096, 4096], P('row', 'col'), may hold values from -6 to 6
- norm_gain: float32 [4096], replicated, may hold values from 0.1 to 1.9
- out_weight: bfloat16 [4096, 4096], P(None, 'col'), may hold values from -0.09375 to 0.09375
Outputs:
- mixed: bfloat16 [4096, 4096], P('row', 'col')
All inputs are finite; a program needn't handle non-finite values.
Results may differ from a plain program's by a relative error of at most 0.015.
Values may be sent and summed in bfloat16 or wider, within the bound.
A program may use at most 64 MiB of HBM per device.

v0:
```python
import math

import jax
import jax.numpy as jnp
from jax import lax
from jax.sharding import PartitionSpec as P

GROUPS = 4


EPSILON = 1e-06
PRECISE = lax.Precision.HIGHEST


def phases(left_idx, right_idx, period):
    product = left_idx[:, None] * right_idx[None, :] % period
    angles = product.astype(jnp.float32) * (2.0 * math.pi / period)
    return (jnp.cos(angles), jnp.sin(angles))


def split_table(table):
    table_high = table.astype(jnp.bfloat16)
    remainder = table - table_high.astype(jnp.float32)
    table_middle = remainder.astype(jnp.bfloat16)
    table_low = (remainder - table_middle.astype(jnp.float32)).astype(jnp.bfloat16)
    return (table_high, table_middle, table_low)


def on_device(tokens, norm_gain, out_weight):
    row_count = lax.axis_size("row")
    col_count = lax.axis_size("col")
    block_len, local_width = tokens.shape
    full_width = local_width * col_count
    group_len = full_width // GROUPS
    share_len = block_len // col_count
    seq_len = block_len * row_count
    slab_len = full_width // row_count
    col_index = lax.axis_index("col")
    chan_idx = jnp.arange(group_len, dtype=jnp.int32)
    cosines, sines = phases(chan_idx, chan_idx, group_len)
    chan_table = jnp.concatenate([cosines, sines], axis=1) / math.sqrt(group_len)
    table_parts = split_table(chan_table)
    arranged = tokens.reshape(col_count, share_len, local_width)
    portion = lax.all_to_all(arranged, "col", split_axis=0, concat_axis=2, tiled=True)
    item_count = portion.shape[1]
    values = portion.astype(jnp.float32)
    inv_rms = lax.rsqrt(jnp.mean(values * values, axis=-1, keepdims=True) + EPSILON)
    normed = lax.optimization_barrier((values * inv_rms * norm_gain).astype(jnp.bfloat16))
    grouped = normed.reshape(item_count, GROUPS, group_len)
    result = jnp.einsum("pgm,mj->pgj", grouped, table_parts[0], preferred_element_type=jnp.float32)
    result = result + jnp.einsum(
        "pgm,mj->pgj", grouped, table_parts[1], preferred_element_type=jnp.float32
    )
    result = result + jnp.einsum(
        "pgm,mj->pgj", grouped, table_parts[2], preferred_element_type=jnp.float32
    )
    high_idx = jnp.arange(row_count, dtype=jnp.int32)
    high_cos, high_sin = phases(high_idx, high_idx, row_count)
    high_table = jnp.concatenate(
        [jnp.concatenate([high_cos, -high_sin], 1), jnp.concatenate([-high_sin, -high_cos], 1)], 0
    )
    parts = (
        lax.all_to_all(
            result[..., :group_len].reshape(1, item_count, full_width),
            "row",
            split_axis=2,
            concat_axis=0,
            tiled=True,
        ),
        lax.all_to_all(
            result[..., group_len:].reshape(1, item_count, full_width),
            "row",
            split_axis=2,
            concat_axis=0,
            tiled=True,
        ),
    )
    item_count = parts[0].shape[1]
    stacked = jnp.concatenate(parts, 0).reshape(2 * row_count, item_count * slab_len)
    result = jnp.dot(high_table, stacked, precision=PRECISE)
    real_part = result[:row_count].reshape(row_count, item_count, slab_len)
    imag_part = result[row_count:].reshape(row_count, item_count, slab_len)
    local_pos = col_index * share_len + jnp.arange(share_len, dtype=jnp.int32)
    twist_cos, twist_sin = phases(high_idx, local_pos, seq_len)
    twist_cos = twist_cos[:, :, None]
    twist_sin = twist_sin[:, :, None]
    turned_real = real_part * twist_cos + imag_part * twist_sin
    turned_imag = imag_part * twist_cos - real_part * twist_sin
    low_idx = jnp.arange(block_len, dtype=jnp.int32)
    low_cos, low_sin = phases(low_idx, low_idx, block_len)
    low_cos = low_cos / math.sqrt(seq_len)
    low_sin = low_sin / math.sqrt(seq_len)
    low_table = jnp.concatenate([low_cos, low_sin], 1)
    stacked = jnp.concatenate(
        (
            lax.all_to_all(turned_real, "col", split_axis=0, concat_axis=1, tiled=True),
            lax.all_to_all(turned_imag, "col", split_axis=0, concat_axis=1, tiled=True),
        ),
        1,
    )
    finished = (jnp.einsum("ks,asc->akc", low_table, stacked, precision=PRECISE),)[0]
    spectrum = finished.astype(jnp.bfloat16)
    returned = lax.all_to_all(spectrum, "row", split_axis=1, concat_axis=2, tiled=True)
    mapped = jnp.einsum(
        "akd,de->kae",
        lax.all_gather(returned, "col", axis=0, tiled=True),
        out_weight,
        preferred_element_type=jnp.float32,
    )
    return mapped.astype(jnp.bfloat16).reshape(block_len, local_width)


def solution(mesh):
    placed = (P("row", "col"), P(), P(None, "col"))
    return jax.shard_map(
        on_device, mesh=mesh, in_specs=placed, out_specs=P("row", "col"), check_vma=False
    )
```

profile of v0, /device:TPU:17, one launch (start us, length us, event | category | flops | bytes accessed | tf_op | source)
XLA Modules:
  0.0 339.8 jit_solution(3100324161421210881)
XLA Ops:
  6.5 3.5 %all-to-all-start = ((bf16[4,128,1024]{2,1,0:T(8,128)(2,1)}), bf16[4,128,1024]{2,1,0:T(8,128)(2,1)S(1)}, u32[]{:S(2)}, u32[]{:S(2)}) async-start(bf16[4,128,1024]{2,1,0:T(8,128)(2,1)} %bitcast.99), calls=%async_computation | async-start | bytes 2097152 | tf_op jit(solution)/shard_map/all_to_all | solution.py:44
  10.1 17.6 %fusion.34 = (f32[1024,1024]{1,0:T(8,128)}, f32[1024,1024]{1,0:T(8,128)}) fusion(), kind=kLoop, calls=%fused_computation.43 | loop fusion | flops 14680064 | bytes 8388608 | tf_op jit(solution)/shard_map/sin | solution.py:18
  27.6 0.0 copy-start.3
  27.6 0.0 all-to-all-done
  27.6 1.6 convert_bitcast_fusion
  29.3 1.9 copy.49
  31.2 0.0 copy-start
  31.2 0.3 fusion.29
  31.5 0.0 copy-done.3
  31.5 0.9 fusion.33
  32.4 1.0 copy-done
  33.4 0.0 copy-start.1
  33.4 4.7 %fusion.4 = f32[128,4,2048]{2,0,1:T(8,128)S(1)} fusion(bf16[128,4,1024]{0,2,1:T(8,128)(2,1)S(1)} %bitcast.81, f32[1024,1024]{1,0:T(8,128)S(1)} %copy-done, f32[1024,1024]{1,0:T(8,128)} %get-tuple-element.14), kind=kOutput, calls=%fused_computation.10 | convolution fusion | flops 2153775104 | bytes 13631488 | tf_op jit(solution)/shard_map/pgm,mj->pgj/dot_general | solution.py:50
  38.1 0.0 copy-done.1
  38.1 2.4 fusion.10
  40.5 2.5 add_add_fusion
  43.0 1.8 fusion.88
  44.7 1.8 copy.53
  46.6 5.7 %all-to-all-start.1 = ((f32[1,128,4096]{1,0,2:T(1,128)}), f32[1,128,4096]{1,0,2:T(1,128)S(1)}, u32[]{:S(2)}, u32[]{:S(2)}) async-start(f32[1,128,4096]{1,0,2:T(1,128)} %bitcast.90), calls=%async_computation.1 | async-start | bytes 4194304 | tf_op jit(solution)/shard_map/all_to_all | solution.py:63
  52.3 2.9 copy.56
  55.2 42.3 %all-to-all-done.1 = f32[1,128,4096]{1,0,2:T(1,128)S(1)} async-done(((f32[1,128,4096]{1,0,2:T(1,128)}), f32[1,128,4096]{1,0,2:T(1,128)S(1)}, u32[]{:S(2)}, u32[]{:S(2)}) %all-to-all-start.1) | async-done | bytes 2097184 | tf_op jit(solution)/shard_map/all_to_all | solution.py:63
  97.5 8.1 %all-to-all-start.2 = ((f32[1,128,4096]{1,0,2:T(1,128)}), f32[1,128,4096]{1,0,2:T(1,128)}, u32[]{:S(2)}, u32[]{:S(2)}) async-start(f32[1,128,4096]{1,0,2:T(1,128)} %bitcast.87), calls=%async_computation.2 | async-start | bytes 4194304 | tf_op jit(solution)/shard_map/all_to_all | solution.py:70
  105.6 0.1 fusion.78
  105.6 0.1 sine_negate_fusion
  105.7 0.1 fusion.76
  105.7 1.9 copy.55
  107.6 2.8 copy.73
  110.4 40.4 %all-to-all-done.2 = f32[1,128,4096]{1,0,2:T(1,128)} async-done(((f32[1,128,4096]{1,0,2:T(1,128)}), f32[1,128,4096]{1,0,2:T(1,128)}, u32[]{:S(2)}, u32[]{:S(2)}) %all-to-all-start.2) | async-done | bytes 2097184 | tf_op jit(solution)/shard_map/all_to_all | solution.py:70
  150.8 2.9 copy.58
  153.7 2.8 copy.74
  156.5 3.8 %fusion.12 = f32[16,65536]{1,0:T(8,128)S(1)} fusion(f32[8,65536]{1,0:T(8,128)S(1)} %bitcast.85, f32[8,65536]{1,0:T(8,128)S(1)} %bitcast.84, f32[8,8]{1,0:T(8,128)S(1)} %fusion.78, f32[8,8]{1,0:T(8,128)S(1)} %get-tuple-element.15, f32[8,8]{1,0:T(8,128)S(1)} %get-tuple-element.16), kind=kOutput, calls=%fused_computation.16 | convolution fusion | flops 202375936 | bytes 8389376 | tf_op jit(solution)/shard_map/dot_general | solution.py:80
  160.2 0.3 fusion.87
  160.5 3.7 %multiply_add_fusion = (f32[8,128,512]{2,1,0:T(8,128)S(1)}, f32[8,128,512]{2,1,0:T(8,128)}) fusion(f32[8,128,512]{2,0,1:T(8,128)S(1)} %bitcast.92, f32[8,128,512]{2,0,1:T(8,128)S(1)} %bitcast.91, f32[8,128]{1,0:T(8,128)S(1)} %get-tuple-element.12, f32[8,128]{1,0:T(8,128)S(1)} %get-tuple-element.11), kind=kLoop, calls=%fused_computation.42 | loop fusion | flops 3145728 | bytes 8396800 | tf_op jit(solution)/shard_map/add | solution.py:87
  164.2 27.7 %all_to_all.93 = f32[8,128,512]{2,1,0:T(8,128)} all-to-all(f32[8,128,512]{2,1,0:T(8,128)S(1)} %get-tuple-element.5), channel_id=1, replica_groups=mesh['row'=8,'col'=4] {'col'}, dimensions={0} | all-to-all | bytes 4194304 | tf_op jit(solution)/shard_map/all_to_all | solution.py:96
  191.9 3.6 %all-to-all-start.4 = ((f32[8,128,512]{2,1,0:T(8,128)}), f32[8,128,512]{2,1,0:T(8,128)S(1)}, u32[]{:S(2)}, u32[]{:S(2)}) async-start(f32[8,128,512]{2,1,0:T(8,128)} %get-tuple-element.6), calls=%async_computation.4 | async-start | bytes 4194304 | tf_op jit(solution)/shard_map/all_to_all | solution.py:97
  195.5 0.3 all-gather.2.cloned.1.call-start
  195.8 5.3 %sine_multiply_fusion = (f32[512,512]{1,0:T(8,128)S(1)}, f32[512,512]{1,0:T(8,128)}) fusion(), kind=kLoop, calls=%fused_computation.56 | loop fusion | flops 4194304 | bytes 2097152 | tf_op jit(solution)/shard_map/div | solution.py:92
  201.1 2.9 copy.61
  204.1 3.1 all_to_all.78
  207.1 12.8 %all-to-all-done.4 = f32[8,128,512]{2,1,0:T(8,128)S(1)} async-done(((f32[8,128,512]{2,1,0:T(8,128)}), f32[8,128,512]{2,1,0:T(8,128)S(1)}, u32[]{:S(2)}, u32[]{:S(2)}) %all-to-all-start.4) | async-done | bytes 2097184 | tf_op jit(solution)/shard_map/all_to_all | solution.py:97
  219.9 1.8 copy.64
  221.7 0.0 copy-start.2
  221.7 3.2 all_to_all.82
  224.9 0.0 copy-done.2
  224.9 9.6 %fusion.44 = bf16[2,512,512]{1,2,0:T(8,128)(2,1)} fusion(f32[512,512]{1,0:T(8,128)S(1)} %get-tuple-element.17, f32[512,512]{1,0:T(8,128)} %get-tuple-element.18, f32[2,512,512]{1,2,0:T(8,128)} %all_to_all.82, f32[2,512,512]{1,2,0:T(8,128)S(1)} %copy-done.2), kind=kOutput, calls=%fused_computation.50 | convolution fusion | flops 6444548096 | bytes 7340032 | tf_op jit(solution)/shard_map/ks,asc->akc/dot_general | solution.py:101
  234.6 2.5 copy.65
  237.1 30.2 %all_to_all.94 = bf16[2,512,512]{2,0,1:T(2,128)(2,1)S(1)} all-to-all(bf16[2,512,512]{2,0,1:T(2,128)(2,1)S(1)} %copy.65), channel_id=1, replica_groups=mesh['row'=8,'col'=4] {'row'}, dimensions={1} | all-to-all | bytes 2097152 | tf_op jit(solution)/shard_map/all_to_all | solution.py:103
  267.3 0.2 copy.66
  267.5 1.1 copy.72
  268.5 0.0 all-gather.2.cloned.1.call-update
  268.6 53.7 %all-gather.2.cloned.1.call-done = bf16[8,64,4096]{2,1,0:T(8,128)(2,1)} async-done(((bf16[2,64,4096]{2,1,0:T(8,128)(2,1)}), bf16[8,64,4096]{2,1,0:T(8,128)(2,1)}) %all-gather.2.cloned.1.call-update) | async-done | bytes 4194320 | tf_op jit(solution)/shard_map/all_gather | solution.py:106
  322.2 9.1 %fusion.47 = bf16[64,8,1024]{2,0,1:T(8,128)(2,1)S(1)} fusion(bf16[8,64,4096]{2,1,0:T(8,128)(2,1)} %all-gather.2.cloned.1.call-done, bf16[4096,1024]{1,0:T(8,128)(2,1)} %param.5), kind=kOutput, calls=%fused_computation.51 | convolution fusion | flops 4295491584 | bytes 13631488 | tf_op jit(solution)/shard_map/akd,de->kae/dot_general | solution.py:104
  331.4 1.5 copy.80
  (2 shorter events, 0.0 us)
Async XLA Ops:
  6.5 21.1 %all-to-all-start = ((bf16[4,128,1024]{2,1,0:T(8,128)(2,1)}), bf16[4,128,1024]{2,1,0:T(8,128)(2,1)S(1)}, u32[]{:S(2)}, u32[]{:S(2)}) async-start(bf16[4,128,1024]{2,1,0:T(8,128)(2,1)} %bitcast.99), calls=%async_computation | async-start | bytes 2097152 | tf_op jit(solution)/shard_map/all_to_all | solution.py:44
  27.6 3.9 %copy-start.3 = (f32[4096]{0:T(1024)S(1)}, f32[4096]{0:T(1024)}, u32[]{:S(2)}) copy-start(f32[4096]{0:T(1024)} %param.4) | copy-start | bytes 49156
  31.2 2.2 copy-start
  33.4 4.7 %copy-start.1 = (f32[1024,1024]{1,0:T(8,128)S(1)}, f32[1024,1024]{1,0:T(8,128)}, u32[]{:S(2)}) copy-start(f32[1024,1024]{1,0:T(8,128)} %get-tuple-element.14) | copy-start | bytes 12582916
  46.6 50.9 %all-to-all-start.1 = ((f32[1,128,4096]{1,0,2:T(1,128)}), f32[1,128,4096]{1,0,2:T(1,128)S(1)}, u32[]{:S(2)}, u32[]{:S(2)}) async-start(f32[1,128,4096]{1,0,2:T(1,128)} %bitcast.90), calls=%async_computation.1 | async-start | bytes 4194304 | tf_op jit(solution)/shard_map/all_to_all | solution.py:63
  97.5 53.3 %all-to-all-start.2 = ((f32[1,128,4096]{1,0,2:T(1,128)}), f32[1,128,4096]{1,0,2:T(1,128)}, u32[]{:S(2)}, u32[]{:S(2)}) async-start(f32[1,128,4096]{1,0,2:T(1,128)} %bitcast.87), calls=%async_computation.2 | async-start | bytes 4194304 | tf_op jit(solution)/shard_map/all_to_all | solution.py:70
  191.9 28.0 %all-to-all-start.4 = ((f32[8,128,512]{2,1,0:T(8,128)}), f32[8,128,512]{2,1,0:T(8,128)S(1)}, u32[]{:S(2)}, u32[]{:S(2)}) async-start(f32[8,128,512]{2,1,0:T(8,128)} %get-tuple-element.6), calls=%async_computation.4 | async-start | bytes 4194304 | tf_op jit(solution)/shard_map/all_to_all | solution.py:97
  195.5 126.7 %all-gather.2.cloned.1.call-start = ((), (), s32[]{:S(2)}) async-start(), calls=%async_computation.6 | async-start | bytes 5242880 | tf_op jit(solution)/shard_map/all_gather | solution.py:106
  221.7 3.2 copy-start.2
Sparse Core Ops, SparseCore 0:
  268.7 53.5 all-gather.1
where the time goes:
time: 342 us; the launch traced here: 340 us
  waiting for transfers between devices  149 us (44%)
  blocking collectives  57.9 us (17%)
  local copies, waits for them, and re-layouts  36.4 us (11%)
  matrix products  32.1 us (9%)
  other arithmetic  29.6 us (9%)
  starting transfers between devices  21.2 us (6%)
  between operations  13.5 us (4%)
    all_gather x1, waiting for transfers between devices, on_device(): lax.all_gather(returned, 'col', axis=0, tiled=True)  53.7 us
    all_to_all x1, waiting for transfers between devices, on_device(): lax.all_to_all(result[..., :group_len].reshape(1, item_count, full_width)...  42.3 us
    all_to_all x1, waiting for transfers between devices, on_device(): lax.all_to_all(result[..., group_len:].reshape(1, item_count, full_width)...  40.4 us
    all_to_all x1, blocking collectives, on_device(): lax.all_to_all(spectrum, 'row', split_axis=1, concat_axis=2, tiled=True)  30.2 us
    all_to_all x1, blocking collectives, on_device(): lax.all_to_all(turned_real, 'col', split_axis=0, concat_axis=1, tiled=True)  27.7 us
    sin x1, other arithmetic, phases(): return (jnp.cos(angles), jnp.sin(angles))  17.6 us
    all_to_all x1, waiting for transfers between devices, on_device(): lax.all_to_all(turned_imag, 'col', split_axis=0, concat_axis=1, tiled=True)  12.8 us
    dot_general x1, matrix products, on_device(): jnp.einsum('ks,asc->akc', low_table, stacked, precision=PRECISE)  9.62 us
  transfers between devices with their start and end apart: 5, of which 4 were waited for; matrix products, arithmetic and copies ran while one was open for 10% of the time, Pallas kernels for 0%

commit v1 on v0

--- a/solution.py
+++ b/solution.py
@@ -1,4 +1,6 @@
 import math
+
+import numpy as np
 
 import jax
 import jax.numpy as jnp
@@ -24,6 +26,98 @@
     table_middle = remainder.astype(jnp.bfloat16)
     table_low = (remainder - table_middle.astype(jnp.float32)).astype(jnp.bfloat16)
     return (table_high, table_middle, table_low)
+
+
+def host_tables(group_len, row_count, block_len):
+    seq_len = block_len * row_count
+    half = group_len // 2 // row_count
+    slot = np.arange(group_len)
+    freq = (slot // (2 * half)) * half + slot % half
+    odd = slot // half % 2 == 1
+    nyquist = odd & (freq == 0)
+    sine = odd & ~nyquist
+    freq = np.where(nyquist, group_len // 2, freq)
+    chan = np.arange(group_len)
+    angle = 2 * np.pi * (chan[:, None] * freq[None, :] % group_len) / group_len
+    chan_table = np.where(sine[None, :], np.sin(angle), np.cos(angle)) / np.sqrt(group_len)
+    low = np.arange(block_len)
+    angle = 2 * np.pi * (low[:, None] * low[None, :] % block_len) / block_len
+    low_table = np.concatenate([np.cos(angle), np.sin(angle)], 1) / np.sqrt(seq_len)
+    high = np.arange(row_count)
+    angle = 2 * np.pi * (high[:, None] * low[None, :] % seq_len) / seq_len
+    return chan_table, low_table, np.cos(angle), np.sin(angle)
+
+
+def slot_facts(slot, group_len, row_count):
+    half = group_len // 2 // row_count
+    freq = (slot // (2 * half)) * half + slot % half
+    odd = slot // half % 2 == 1
+    nyquist = odd & (freq == 0)
+    return jnp.where(nyquist, group_len // 2, freq), odd & ~nyquist
+
+
+def folding(group_len, row_count):
+    freq, sine = slot_facts(jnp.arange(group_len, dtype=jnp.int32), group_len, row_count)
+    chan = jnp.arange(group_len, dtype=jnp.int32)[None, :]
+    direct = chan == freq[:, None]
+    mirror = chan == ((group_len - freq) % group_len)[:, None]
+    signed = jnp.where(sine[:, None], -1.0, 1.0)
+    return jnp.where(direct, signed, jnp.where(mirror, 1.0, 0.0)).astype(jnp.bfloat16)
+
+
+def on_device_folded(tokens, norm_gain, out_weight):
+    row_count = lax.axis_size("row")
+    col_count = lax.axis_size("col")
+    block_len, group_len = tokens.shape
+    full_width = group_len * col_count
+    slab = group_len // row_count
+    out_width = out_weight.shape[1]
+    chan_table, low_table, twist_cos, twist_sin = host_tables(group_len, row_count, block_len)
+    chan_table = jnp.asarray(chan_table, jnp.bfloat16)
+    low_table = jnp.asarray(low_table, jnp.bfloat16)
+    twist_cos = jnp.asarray(twist_cos, jnp.float32)[:, :, None]
+    twist_sin = jnp.asarray(twist_sin, jnp.float32)[:, :, None]
+    values = tokens.astype(jnp.float32)
+    total = lax.psum(jnp.sum(values * values, axis=-1), "col")
+    inv_rms = lax.rsqrt(total / full_width + EPSILON)[:, None]
+    gain = lax.dynamic_slice_in_dim(norm_gain, lax.axis_index("col") * group_len, group_len)
+    normed = (values * inv_rms * gain).astype(jnp.bfloat16)
+    chans = jnp.dot(normed, chan_table, preferred_element_type=jnp.float32).astype(jnp.bfloat16)
+    moved = lax.all_to_all(chans, "row", split_axis=1, concat_axis=0, tiled=True)
+    blocks = moved.reshape(row_count, block_len, slab).astype(jnp.float32)
+    _, sine = slot_facts(
+        lax.axis_index("row") * slab + jnp.arange(slab, dtype=jnp.int32), group_len, row_count
+    )
+    tops, bottoms = [], []
+    for q in range(row_count):
+        real, imag = 0.0, 0.0
+        for a in range(row_count):
+            angle = 2 * math.pi * (a * q % row_count) / row_count
+            real = real + blocks[a] * round(math.cos(angle), 12)
+            imag = imag - blocks[a] * round(math.sin(angle), 12)
+        turned_real = real * twist_cos[q] + imag * twist_sin[q]
+        turned_imag = imag * twist_cos[q] - real * twist_sin[q]
+        tops.append(jnp.where(sine, -turned_imag, turned_real).astype(jnp.bfloat16))
+        bottoms.append(jnp.where(sine, turned_real, turned_imag).astype(jnp.bfloat16))
+    stacked = jnp.concatenate([jnp.concatenate(tops, 1), jnp.concatenate(bottoms, 1)], 0)
+    lows = jnp.dot(low_table, stacked, preferred_element_type=jnp.float32).astype(jnp.bfloat16)
+    back = lax.all_to_all(
+        lows.reshape(row_count, block_len // row_count, row_count * slab),
+        "row", split_axis=0, concat_axis=0, tiled=True,
+    )
+    gathered = lax.all_gather(back, "col", axis=0, tiled=False)
+    fold = folding(group_len, row_count)
+    folded = jnp.einsum(
+        "sm,gme->gse", fold, out_weight.reshape(col_count, group_len, out_width),
+        preferred_element_type=jnp.float32,
+    ).astype(jnp.bfloat16)
+    mapped = jnp.einsum(
+        "gspql,gsle->pqe",
+        gathered.reshape(col_count, row_count, block_len // row_count, row_count, slab),
+        folded.reshape(col_count, row_count, slab, out_width),
+        preferred_element_type=jnp.float32,
+    )
+    return mapped.astype(jnp.bfloat16).reshape(block_len, out_width)
 
 
 def on_device(tokens, norm_gain, out_weight):
@@ -111,7 +205,12 @@
 
 
 def solution(mesh):
+    def body(tokens, norm_gain, out_weight):
+        whole_groups = tokens.shape[1] * GROUPS == out_weight.shape[0]
+        program = on_device_folded if whole_groups else on_device
+        return program(tokens, norm_gain, out_weight)
+
     placed = (P("row", "col"), P(), P(None, "col"))
     return jax.shard_map(
-        on_device, mesh=mesh, in_specs=placed, out_specs=P("row", "col"), check_vma=False
-    )
+        body, mesh=mesh, in_specs=placed, out_specs=P("row", "col"), check_vma=False
+    )

time: 342 us -> 160 us (0.47)
  waiting for transfers between devices: 149 us -> 60.7 us
  local copies, waits for them, and re-layouts: 36.4 us -> 7.33 us
  other arithmetic: 29.6 us -> 6.34 us
  blocking collectives: 57.9 us -> 37.4 us
  starting transfers between devices: 21.2 us -> 7.5 us
  matrix products: 32.1 us -> 25 us
    all_to_all x4 -> x1, waiting for transfers between devices: 95.4 us -> 22.7 us  [on_device_folded(): lax.all_to_all(chans, 'row', split_axis=1, concat_axis=0, tiled=True)]
    all_to_all x2 -> x1, blocking collectives: 57.9 us -> 29.5 us  [on_device_folded(): lax.all_to_all(lows.reshape(row_count, block_len // row_count, row_count...]
    sin x1 -> x0, other arithmetic: 17.6 us -> none  [phases(): return (jnp.cos(angles), jnp.sin(angles))]
    all_to_all x8 -> x1, local copies, waits for them, and re-layouts: 17.1 us -> 1.16 us  [on_device_folded(): lax.all_to_all(chans, 'row', split_axis=1, concat_axis=0, tiled=True)]
    all_gather x1, waiting for transfers between devices: 53.7 us -> 38 us  [on_device_folded(): gathered = lax.all_gather(back, 'col', axis=0, tiled=False)]
    all_to_all x4 -> x1, starting transfers between devices: 20.9 us -> 7.49 us  [on_device_folded(): lax.all_to_all(chans, 'row', split_axis=1, concat_axis=0, tiled=True)]
    psum x0 -> x1, blocking collectives: none -> 7.89 us  [on_device_folded(): total = lax.psum(jnp.sum(values * values, axis=-1), 'col')]
    dot_general x6 -> x5, matrix products: 32.1 us -> 25 us  [the longest x1 14.8 us: on_device_folded(): jnp.einsum('sm,gme->gse', fold, out_weight.reshape(col_count, group_len,...]
  transfers between devices with their start and end apart: 5 -> 2, of which waited for: 4 -> 2; matrix products, arithmetic and copies ran while one was open for 10% -> 9% of each run, Pallas kernels for 0% -> 0%
where the time goes in v1:
time: 160 us; the launch traced here: 158 us
  waiting for transfers between devices  60.7 us (38%)
  blocking collectives  37.4 us (23%)
  matrix products  25 us (16%)
  between operations  13.6 us (8%)
  starting transfers between devices  7.5 us (5%)
  local copies, waits for them, and re-layouts  7.33 us (5%)
  other arithmetic  6.34 us (4%)
    all_gather x1, waiting for transfers between devices, on_device_folded(): gathered = lax.all_gather(back, 'col', axis=0, tiled=False)  38 us
    all_to_all x1, blocking collectives, on_device_folded(): lax.all_to_all(lows.reshape(row_count, block_len // row_count, row_count...  29.5 us
    all_to_all x1, waiting for transfers between devices, on_device_folded(): lax.all_to_all(chans, 'row', split_axis=1, concat_axis=0, tiled=True)  22.7 us
    dot_general x1, matrix products, on_device_folded(): jnp.einsum('sm,gme->gse', fold, out_weight.reshape(col_count, group_len,...  14.8 us
    psum x1, blocking collectives, on_device_folded(): total = lax.psum(jnp.sum(values * values, axis=-1), 'col')  7.89 us
    all_to_all x1, starting transfers between devices, on_device_folded(): lax.all_to_all(chans, 'row', split_axis=1, concat_axis=0, tiled=True)  7.49 us
    dot_general x1, matrix products, on_device_folded(): jnp.einsum('gspql,gsle->pqe', gathered.reshape(col_count, row_count, bloc...  5.52 us
    unnamed x35, local copies, waits for them, and re-layouts  5.47 us
  transfers between devices with their start and end apart: 2, of which 2 were waited for; matrix products, arithmetic and copies ran while one was open for 9% of the time, Pallas kernels for 0%

profile of v1, /device:TPU:17, one launch (start us, length us, event | category | flops | bytes accessed | tf_op | source)
XLA Modules:
  0.0 157.9 jit_solution(6261747024273125081)
XLA Ops:
  6.5 1.5 fusion
  8.0 7.9 %psum.7 = f32[512]{0:T(512)S(1)} all-reduce(f32[512]{0:T(512)S(1)} %fusion), channel_id=1, replica_groups=mesh['row'=8,'col'=4] {'col'}, use_global_device_ids=true, to_apply=%region_1.0 | all-reduce | flops 512 | bytes 4096 | tf_op jit(solution)/shard_map/psum | solution.py:81
  15.9 0.7 dynamic_slice.3
  16.6 3.2 %fusion.10 = bf16[64,8,8,128]{3,2,1,0:T(8,128)(2,1)S(1)} fusion(bf16[1024,1024]{1,0:T(8,128)(2,1)} %constant.151.clone, bf16[512,1024]{1,0:T(8,128)(2,1)} %param.7, f32[1024]{0:T(1024)S(1)} %dynamic_slice.3, f32[512]{0:T(512)S(1)} %add_rsqrt_fusion), kind=kOutput, calls=%fused_computation.19 | convolution fusion | flops 1076363264 | bytes 4200448 | tf_op jit(solution)/shard_map/dot_general | solution.py:85
  19.9 1.2 copy.26
  21.0 7.5 %all-to-all-start = ((bf16[512,8,128]{2,0,1:T(8,128)(2,1)}), bf16[512,8,128]{2,0,1:T(8,128)(2,1)S(1)}, u32[]{:S(2)}, u32[]{:S(2)}) async-start(bf16[512,8,128]{2,0,1:T(8,128)(2,1)} %bitcast.434), calls=%async_computation | async-start | bytes 2097152 | tf_op jit(solution)/shard_map/all_to_all | solution.py:86
  28.5 0.0 all-gather.3.cloned.1.call-start
  28.6 22.7 %all-to-all-done = bf16[512,8,128]{2,0,1:T(8,128)(2,1)S(1)} async-done(((bf16[512,8,128]{2,0,1:T(8,128)(2,1)}), bf16[512,8,128]{2,0,1:T(8,128)(2,1)S(1)}, u32[]{:S(2)}, u32[]{:S(2)}) %all-to-all-start) | async-done | bytes 1048608 | tf_op jit(solution)/shard_map/all_to_all | solution.py:86
  51.2 0.1 convert_bitcast_fusion
  51.4 0.0 copy-start.14
  51.4 0.0 copy-start.15
  51.4 0.0 copy-start.8
  51.4 0.0 copy-start.9
  51.4 0.3 fusion.23
  51.7 0.4 copy-done.14
  52.1 0.0 copy-done.15
  52.1 0.0 copy-start.6
  52.1 0.0 copy-start.7
  52.1 0.4 fusion.24
  52.5 0.0 copy-done.8
  52.5 0.0 copy-done.9
  52.5 0.0 copy-start.12
  52.5 0.0 copy-start.13
  52.5 0.4 fusion.25
  52.9 0.0 copy-done.6
  52.9 0.0 copy-done.7
  52.9 0.4 fusion.26
  53.3 0.0 copy-start.4
  53.4 0.0 copy-start.5
  53.4 0.0 copy-done.12
  53.4 0.0 copy-done.13
  53.4 0.3 fusion.27
  53.7 0.0 copy-start.2
  53.7 0.0 copy-start.3
  53.7 0.3 copy-done.4
  54.0 0.0 copy-done.5
  54.0 0.0 copy-start.10
  54.0 0.0 copy-start.11
  54.0 0.4 fusion.28
  54.4 0.0 copy-done.2
  54.5 0.0 copy-done.3
  54.5 0.4 fusion.29
  54.9 0.0 copy-done.10
  54.9 0.0 copy-done.11
  54.9 0.5 fusion.30
  55.4 0.0 copy-start.1
  55.4 0.3 fusion.17
  55.7 0.3 fusion.18
  55.9 0.3 fusion.19
  56.2 0.3 fusion.20
  56.5 0.3 fusion.21
  56.7 0.0 copy-start
  56.8 0.3 fusion.22
  57.0 0.0 copy-done.1
  57.0 0.7 fusion.50
  57.7 0.0 copy-done
  57.8 0.7 add_convert_fusion
  58.5 29.5 %all_to_all.18 = bf16[8,64,1024]{2,1,0:T(8,128)(2,1)} all-to-all(bf16[8,64,1024]{2,1,0:T(8,128)(2,1)S(1)} %bitcast.437), channel_id=1, replica_groups=mesh['row'=8,'col'=4] {'row'}, dimensions={0} | all-to-all | bytes 2097152 | tf_op jit(solution)/shard_map/all_to_all | solution.py:104
  88.0 0.0 all-gather.3.cloned.1.call-update
  88.1 14.8 %convolution_convert_fusion = bf16[1024,4,1024]{2,0,1:T(8,128)(2,1)} fusion(bf16[4,1024,1024]{2,1,0:T(8,128)(2,1)} %bitcast.438, s32[1024]{0:T(1024)S(1)} %get-tuple-element.30, bf16[1024]{0:T(1024)(128)(2,1)S(1)} %and_select_fusion, s32[1024]{0:T(1024)S(1)} %get-tuple-element.31), kind=kOutput, calls=%fused_computation | convolution fusion | flops 8598323200 | bytes 16787456 | tf_op jit(solution)/shard_map/sm,gme->gse/dot_general | solution.py:110
  102.9 38.0 %all-gather.3.cloned.1.call-done = bf16[32,64,1024]{2,1,0:T(8,128)(2,1)} async-done(((bf16[8,64,1024]{2,1,0:T(8,128)(2,1)}), bf16[32,64,1024]{2,1,0:T(8,128)(2,1)}) %all-gather.3.cloned.1.call-update) | async-done | bytes 4194320 | tf_op jit(solution)/shard_map/all_gather | solution.py:108
  140.9 3.5 %copy.24 = bf16[256,8,8,128]{3,2,1,0:T(8,128)(2,1)S(1)} copy(bf16[256,8,8,128]{3,1,2,0:T(8,128)(2,1)} %bitcast.435) | data formatting | bytes 8388608
  144.4 1.1 copy-done.16
  145.5 5.5 %fusion.11 = bf16[512,1024]{1,0:T(8,128)(2,1)} fusion(bf16[4,8,64,8,128]{4,3,2,1,0:T(8,128)(2,1)S(1)} %bitcast.436, bf16[4,8,128,1024,1]{3,2,4,1,0:T(8,128)(2,1)S(1)} %bitcast.439), kind=kOutput, calls=%fused_computation.20 | convolution fusion | flops 4295491584 | bytes 13631488 | tf_op jit(solution)/shard_map/gspql,gsle->pqe/dot_general | solution.py:114
  (5 shorter events, 0.1 us)
Async XLA Ops:
  21.0 30.2 %all-to-all-start = ((bf16[512,8,128]{2,0,1:T(8,128)(2,1)}), bf16[512,8,128]{2,0,1:T(8,128)(2,1)S(1)}, u32[]{:S(2)}, u32[]{:S(2)}) async-start(bf16[512,8,128]{2,0,1:T(8,128)(2,1)} %bitcast.434), calls=%async_computation | async-start | bytes 2097152 | tf_op jit(solution)/shard_map/all_to_all | solution.py:86
  28.5 112.4 %all-gather.3.cloned.1.call-start = ((), (), s32[]{:S(2)}) async-start(), calls=%async_computation.2 | async-start | bytes 5242880 | tf_op jit(solution)/shard_map/all_gather | solution.py:108
  51.4 0.7 copy-start.14
  51.4 0.7 copy-start.15
  51.4 1.1 copy-start.8
  51.4 1.1 copy-start.9
  52.1 0.8 copy-start.6
  52.1 0.8 copy-start.7
  52.5 0.9 copy-start.12
  52.5 0.9 copy-start.13
  53.3 0.7 copy-start.4
  53.4 0.7 copy-start.5
  53.7 0.8 copy-start.2
  53.7 0.8 copy-start.3
  54.0 0.8 copy-start.10
  54.0 0.8 copy-start.11
  55.4 1.6 %copy-start.1 = (bf16[512,512]{1,0:T(8,128)(2,1)S(1)}, bf16[512,512]{1,0:T(8,128)(2,1)}, u32[]{:S(2)}) copy-start(bf16[512,512]{1,0:T(8,128)(2,1)} %constant.187) | copy-start | bytes 1572868
  56.7 1.0 copy-start
  140.9 4.6 %copy-start.16 = (bf16[1024,4,1024]{2,0,1:T(8,128)(2,1)S(1)}, bf16[1024,4,1024]{2,0,1:T(8,128)(2,1)}, u32[]{:S(2)}) copy-start(bf16[1024,4,1024]{2,0,1:T(8,128)(2,1)} %convolution_convert_fusion) | copy-start | bytes 25165828
Sparse Core Ops, SparseCore 0:
  88.2 52.6 all-gather.2

commit v2 on v1

--- a/solution.py
+++ b/solution.py
@@ -1,3 +1,4 @@
+import functools
 import math
 
 import numpy as np
@@ -5,6 +6,8 @@
 import jax
 import jax.numpy as jnp
 from jax import lax
+from jax.experimental import pallas as pl
+from jax.experimental.pallas import tpu as pltpu
 from jax.sharding import PartitionSpec as P
 
 GROUPS = 4
@@ -118,6 +121,331 @@
         preferred_element_type=jnp.float32,
     )
     return mapped.astype(jnp.bfloat16).reshape(block_len, out_width)
+
+
+MESH = pl.DeviceIdType.MESH
+F32 = jnp.float32
+BF16 = jnp.bfloat16
+
+
+def fused_kernel(
+    dims, x_ref, gain_ref, table_ref, low_ref, twist_ref, w_hbm, out_ref,
+    w_ref, fold_ref, folded, send1, recv1, sums, stacked, send2, lhs, acc, spread,
+    w_sem, s_send, s_recv, a_send, a_recv, b_send, b_recv, g_send, g_recv, l_sem,
+):
+    row_count, col_count = dims
+    block_len, group_len = x_ref.shape
+    full_width = group_len * col_count
+    slab = group_len // row_count
+    half = slab // 2
+    pair = 2 * slab
+    chips = row_count // 2
+    part = block_len // row_count
+    out_width = out_ref.shape[1]
+    r = lax.axis_index("row")
+    c = lax.axis_index("col")
+    z = r // 2
+    other = 2 * z + 1 - r % 2
+    x_next = 2 * (c // 2) + 1 - c % 2
+    y_next = 2 * (1 - c // 2) + c % 2
+    diagonal = 2 * (1 - c // 2) + 1 - c % 2
+    col_peers = (x_next, y_next, diagonal)
+    w_copy = pltpu.make_async_copy(w_hbm, w_ref, w_sem)
+    w_copy.start()
+
+    barrier = pltpu.get_barrier_semaphore()
+    for step in range(1, row_count):
+        pl.semaphore_signal(
+            barrier, inc=1, device_id=(lax.rem(r + step, row_count), c), device_id_type=MESH
+        )
+    for peer in col_peers:
+        pl.semaphore_signal(barrier, inc=1, device_id=(r, peer), device_id_type=MESH)
+    pl.semaphore_wait(barrier, row_count + col_count - 2)
+
+    values = x_ref[...].astype(F32)
+    squares = values * values
+    top = squares.astype(BF16)
+    rest = (squares - top.astype(F32)).astype(BF16)
+    ones = jnp.ones((16, group_len), BF16)
+    lanes = (((1,), (1,)), ((), ()))
+    own = lax.dot_general(ones, top, lanes, preferred_element_type=F32)
+    own = own + lax.dot_general(ones, rest, lanes, preferred_element_type=F32)
+    sums[c] = own[:8]
+    sum_copies = []
+    for k, peer in enumerate(col_peers):
+        copy = pltpu.make_async_remote_copy(
+            src_ref=sums.at[c], dst_ref=sums.at[c], send_sem=s_send.at[k], recv_sem=s_recv.at[k],
+            device_id=(r, peer), device_id_type=MESH,
+        )
+        copy.start()
+        sum_copies.append(copy)
+
+    gain = gain_ref[:, pl.ds(pl.multiple_of(c * group_len, group_len), group_len)]
+    scaled = (values * gain).astype(BF16)
+    far_first = sorted(range(chips), key=lambda d: -min(d, chips - d))
+    first_copies = []
+    inv = None
+    for d in far_first:
+        chip = lax.rem(z + d, chips)
+        product = jnp.dot(
+            scaled, table_ref[:, pl.ds(pl.multiple_of(chip * pair, pair), pair)],
+            preferred_element_type=F32,
+        )
+        if inv is None:
+            for copy in sum_copies:
+                copy.wait_recv()
+            total = sums[0, :1, :]
+            for k in range(1, col_count):
+                total = total + sums[k, :1, :]
+            inv = lax.rsqrt(total / full_width + EPSILON)
+            inv = jnp.transpose(jnp.broadcast_to(inv, (128, block_len)))
+        send1[2 * chip] = (product[:, :slab] * inv).astype(BF16)
+        send1[2 * chip + 1] = (product[:, slab:] * inv).astype(BF16)
+        for target, slot in ([(2 * chip, 2 * d), (2 * chip + 1, 2 * d + 1)] if d else [(other, 0)]):
+            copy = pltpu.make_async_remote_copy(
+                src_ref=send1.at[target], dst_ref=recv1.at[r], send_sem=a_send.at[slot],
+                recv_sem=a_recv.at[slot] if d == 0 else a_recv.at[2 * d + r % 2],
+                device_id=(target, c), device_id_type=MESH,
+            )
+            copy.start()
+            first_copies.append(copy)
+    stay1 = pltpu.make_async_copy(send1.at[r], recv1.at[r], l_sem.at[0])
+    stay1.start()
+
+    for t in range(chips):
+        slot = t * pair + lax.broadcasted_iota(jnp.int32, (pair, 4 * slab), 0)
+        column = lax.broadcasted_iota(jnp.int32, (pair, 4 * slab), 1)
+        within = slot % slab
+        freq = (slot // slab) * half + within % half
+        odd = within >= half
+        nyquist = odd & (freq == 0)
+        high = min(group_len - slab * (t + 1), group_len - pair)
+        direct = (column == freq - slab * t) & ~nyquist & (column < slab)
+        mirror = (column - slab + high == group_len - freq) & (freq > 0)
+        mirror = mirror & (column >= slab) & (column < 3 * slab)
+        middle = nyquist & (column == 3 * slab)
+        signed = jnp.where(odd, -1.0, 1.0)
+        fold_ref[t] = jnp.where(direct, signed, jnp.where(mirror | middle, 1.0, 0.0)).astype(BF16)
+
+    w_copy.wait()
+    wide = 256
+    pieces = out_width // wide
+
+    def fold_step(i, carry):
+        base = pl.multiple_of((i // pieces) * group_len, group_len)
+        cols = pl.ds(pl.multiple_of((i % pieces) * wide, wide), wide)
+        for t in range(chips):
+            high = min(group_len - slab * (t + 1), group_len - pair)
+            taken = [w_ref[pl.ds(base + slab * t, slab), cols], w_ref[pl.ds(base + high, pair), cols]]
+            if t == 0:
+                taken.append(w_ref[pl.ds(base + group_len // 2, slab), cols])
+            depth = slab * (4 if t == 0 else 3)
+            folded[pl.ds(base + pair * t, pair), cols] = jnp.dot(
+                fold_ref[t, :, :depth], jnp.concatenate(taken, 0), preferred_element_type=F32
+            ).astype(BF16)
+        return carry
+
+    lax.fori_loop(0, col_count * pieces, fold_step, 0)
+
+    def arrived(ref, semaphore):
+        pltpu.make_async_remote_copy(
+            src_ref=ref, dst_ref=ref, send_sem=l_sem.at[0], recv_sem=semaphore,
+            device_id=(other, c), device_id_type=MESH,
+        ).wait_recv()
+
+    def block_of(d, i):
+        return 2 * lax.rem(z - d + chips, chips) + i
+
+    stay1.wait()
+    arrived(recv1.at[other], a_recv.at[0])
+    for d in range(1, chips):
+        for i in range(2):
+            arrived(recv1.at[block_of(d, i)], a_recv.at[2 * d + i])
+    tile = 32
+    lane = lax.broadcasted_iota(jnp.int32, (tile, slab), 1)
+    sine = (lane > half) | ((lane == half) & (r > 0))
+
+    def turn_step(i, carry):
+        rows = pl.ds(pl.multiple_of(i * tile, tile), tile)
+        below = pl.ds(pl.multiple_of(block_len + i * tile, tile), tile)
+        blocks = [recv1[a, rows, :].astype(F32) for a in range(row_count)]
+        middle = row_count // 2
+        even = [blocks[a] + blocks[row_count - a] for a in range(1, middle)]
+        odd = [blocks[a] - blocks[row_count - a] for a in range(1, middle)]
+        ends = (blocks[0] + blocks[middle], blocks[0] - blocks[middle])
+        twist = twist_ref[rows, :]
+        for q in range(middle + 1):
+            real = ends[q % 2]
+            imag = None
+            for a in range(1, middle):
+                angle = 2 * math.pi * (a * q % row_count) / row_count
+                cosine, sinus = round(math.cos(angle), 12), round(math.sin(angle), 12)
+                if cosine:
+                    real = real + even[a - 1] * cosine
+                if sinus:
+                    term = odd[a - 1] * -sinus
+                    imag = term if imag is None else imag + term
+            for k, sign in ((q, 1.0), (row_count - q, -1.0)):
+                if k == row_count or (sign < 0 and k == q):
+                    continue
+                cosine, sinus = twist[:, k : k + 1], twist[:, row_count + k : row_count + k + 1]
+                if imag is None:
+                    turned_real, turned_imag = real * cosine, -(real * sinus)
+                else:
+                    turned_real = real * cosine + imag * (sinus * sign)
+                    turned_imag = imag * (cosine * sign) - real * sinus
+                cols = pl.ds(k * slab, slab)
+                stacked[rows, cols] = jnp.where(sine, -turned_imag, turned_real).astype(BF16)
+                stacked[below, cols] = jnp.where(sine, turned_real, turned_imag).astype(BF16)
+        return carry
+
+    lax.fori_loop(0, block_len // tile, turn_step, 0)
+
+    def lanes_of(index):
+        return pl.ds(pl.multiple_of(index * slab, slab), slab)
+
+    second_copies = {}
+    for d in far_first:
+        chip = lax.rem(z + d, chips)
+        lows = jnp.dot(
+            low_ref[pl.ds(pl.multiple_of(chip * 2 * part, 2 * part), 2 * part), :], stacked[...],
+            preferred_element_type=F32,
+        ).astype(BF16)
+        for i in range(2):
+            for q in range(row_count):
+                send2[2 * chip + i, q] = lows[i * part : (i + 1) * part, q * slab : (q + 1) * slab]
+        for target, slot in ([(2 * chip, 2 * d), (2 * chip + 1, 2 * d + 1)] if d else [(other, 0)]):
+            copy = pltpu.make_async_remote_copy(
+                src_ref=send2.at[target], dst_ref=lhs.at[c, :, :, lanes_of(r)],
+                send_sem=b_send.at[slot],
+                recv_sem=b_recv.at[slot] if d == 0 else b_recv.at[2 * d + r % 2],
+                device_id=(target, c), device_id_type=MESH,
+            )
+            copy.start()
+            second_copies[slot] = copy
+    stay2 = pltpu.make_async_copy(send2.at[r], lhs.at[c, :, :, lanes_of(r)], l_sem.at[1])
+    stay2.start()
+
+    sends = []
+
+    def share(origin, source, block, target, out_slot, in_slot):
+        copy = pltpu.make_async_remote_copy(
+            src_ref=source, dst_ref=lhs.at[origin, :, :, lanes_of(block)],
+            send_sem=g_send.at[out_slot], recv_sem=g_recv.at[in_slot],
+            device_id=(r, target), device_id_type=MESH,
+        )
+        copy.start()
+        sends.append(copy)
+        return copy
+
+    def held(origin, block):
+        return lhs.at[origin, :, :, lanes_of(block)]
+
+    order = [(None, r), (None, other)]
+    for d in sorted(range(1, chips), key=lambda d: min(d, chips - d)):
+        order += [((2 * d + i), block_of(d, i)) for i in range(2)]
+    count = len(order)
+    from_x, from_y, from_far = [], [], []
+    for n in range(count + 1):
+        if n < count:
+            slot, block = order[n]
+            if n == 0:
+                stay2.wait()
+            else:
+                arrived(held(c, block), b_recv.at[0 if n == 1 else slot])
+            source = held(c, block)
+            from_x.append(share(c, source, block, x_next, n, n))
+            from_y.append(share(c, source, block, y_next, count + n, count + n))
+        if n:
+            _, block = order[n - 1]
+            slot = 2 * count + n - 1
+            if n % 2:
+                from_x[n - 1].wait_recv()
+                from_far.append(share(x_next, held(x_next, block), block, y_next, slot, slot))
+            else:
+                from_y[n - 1].wait_recv()
+                from_far.append(share(y_next, held(y_next, block), block, x_next, slot, slot))
+
+    def multiply(origin, first, last):
+        base = pl.multiple_of(origin * group_len, group_len)
+
+        def step(i, carry):
+            cols = pl.ds(pl.multiple_of(i * wide, wide), wide)
+            left = lhs[origin].reshape(block_len, group_len)
+            value = jnp.dot(left, folded[pl.ds(base, group_len), cols], preferred_element_type=F32)
+            if not first:
+                value = acc[:, cols] + value
+            if not last:
+                acc[:, cols] = value
+            else:
+                for q in range(row_count):
+                    for j in range(wide // 128):
+                        spread[j, pl.ds(q, part, stride=row_count), :] = value[
+                            q * part : (q + 1) * part, j * 128 : (j + 1) * 128
+                        ]
+                for j in range(wide // 128):
+                    at = pl.ds(pl.multiple_of(i * wide + j * 128, 128), 128)
+                    out_ref[:, at] = spread[j].astype(BF16)
+            return carry
+
+        lax.fori_loop(0, pieces, step, 0)
+
+    multiply(c, True, False)
+    for n in range(1, count, 2):
+        from_x[n].wait_recv()
+    multiply(x_next, False, False)
+    for n in range(0, count, 2):
+        from_y[n].wait_recv()
+    multiply(y_next, False, False)
+    for copy in from_far:
+        copy.wait_recv()
+    multiply(diagonal, False, True)
+
+    for copy in sum_copies + first_copies + list(second_copies.values()) + sends:
+        copy.wait_send()
+
+
+def on_device_fused(tokens, norm_gain, out_weight):
+    row_count = lax.axis_size("row")
+    col_count = lax.axis_size("col")
+    block_len, group_len = tokens.shape
+    out_width = out_weight.shape[1]
+    slab = group_len // row_count
+    part = block_len // row_count
+    chan_table, low_table, twist_cos, twist_sin = host_tables(group_len, row_count, block_len)
+    twist = np.zeros((block_len, 128), np.float32)
+    twist[:, :row_count] = twist_cos.T
+    twist[:, row_count : 2 * row_count] = twist_sin.T
+    vmem = pl.BlockSpec(memory_space=pltpu.VMEM)
+    dma = pltpu.SemaphoreType.DMA
+    return pl.pallas_call(
+        functools.partial(fused_kernel, (row_count, col_count)),
+        out_shape=jax.ShapeDtypeStruct((block_len, out_width), BF16),
+        in_specs=[vmem] * 5 + [pl.BlockSpec(memory_space=pl.ANY)],
+        out_specs=vmem,
+        scratch_shapes=[
+            pltpu.VMEM(out_weight.shape, BF16),
+            pltpu.VMEM((row_count // 2, 2 * slab, 4 * slab), BF16),
+            pltpu.VMEM(out_weight.shape, BF16),
+            pltpu.VMEM((row_count, block_len, slab), BF16),
+            pltpu.VMEM((row_count, block_len, slab), BF16),
+            pltpu.VMEM((col_count, 8, block_len), F32),
+            pltpu.VMEM((2 * block_len, row_count * slab), BF16),
+            pltpu.VMEM((row_count, row_count, part, slab), BF16),
+            pltpu.VMEM((col_count, row_count, part, group_len), BF16),
+            pltpu.VMEM((block_len, out_width), F32),
+            pltpu.VMEM((2, block_len, 128), F32),
+            dma, dma((col_count - 1,)), dma((col_count - 1,)),
+            dma((row_count,)), dma((row_count,)), dma((row_count,)), dma((row_count,)),
+            dma((3 * row_count,)), dma((3 * row_count,)), dma((2,)),
+        ],
+        compiler_params=pltpu.CompilerParams(
+            collective_id=0, has_side_effects=True, vmem_limit_bytes=60 * 1024 * 1024
+        ),
+    )(
+        tokens, norm_gain[None, :], jnp.asarray(chan_table, BF16), jnp.asarray(low_table, BF16),
+        jnp.asarray(twist), out_weight,
+    )
 
 
 def on_device(tokens, norm_gain, out_weight):
@@ -207,7 +535,10 @@
 def solution(mesh):
     def body(tokens, norm_gain, out_weight):
         whole_groups = tokens.shape[1] * GROUPS == out_weight.shape[0]
+        slab = tokens.shape[1] // mesh.shape["row"]
         program = on_device_folded if whole_groups else on_device
+        if whole_groups and slab == 128 and mesh.shape["col"] == 4 and mesh.shape["row"] == 8:
+            program = on_device_fused
         return program(tokens, norm_gain, out_weight)
 
     placed = (P("row", "col"), P(), P(None, "col"))

time: 160 us -> 91.5 us (0.57); the launches traced: 158 us -> 91.4 us
  Pallas kernels: 0 us -> 89.1 us
  waiting for transfers between devices: 60.7 us -> 0 us
  blocking collectives: 37.4 us -> 0 us
  matrix products: 25 us -> 0 us
  between operations: 13.6 us -> 0.01 us
  starting transfers between devices: 7.5 us -> 0 us
  other arithmetic: 6.34 us -> 0 us
  local copies, waits for them, and re-layouts: 7.33 us -> 2.26 us
    pallas_call x0 -> x1, Pallas kernels: none -> 89.1 us  [on_device_fused(): pl.pallas_call(functools.partial(fused_kernel, (row_count, col_count)), o...]
    all_gather x1 -> x0, waiting for transfers between devices: 38 us -> none  [on_device_folded(): gathered = lax.all_gather(back, 'col', axis=0, tiled=False)]
    all_to_all x1 -> x0, blocking collectives: 29.5 us -> none  [on_device_folded(): lax.all_to_all(lows.reshape(row_count, block_len // row_count, row_count...]
    dot_general x5 -> x0, matrix products: 25 us -> none  [the longest x1 14.8 us: on_device_folded(): jnp.einsum('sm,gme->gse', fold, out_weight.reshape(col_count, group_len,...]
    all_to_all x1 -> x0, waiting for transfers between devices: 22.7 us -> none  [on_device_folded(): lax.all_to_all(chans, 'row', split_axis=1, concat_axis=0, tiled=True)]
    psum x1 -> x0, blocking collectives: 7.89 us -> none  [on_device_folded(): total = lax.psum(jnp.sum(values * values, axis=-1), 'col')]
    all_to_all x1 -> x0, starting transfers between devices: 7.49 us -> none  [on_device_folded(): lax.all_to_all(chans, 'row', split_axis=1, concat_axis=0, tiled=True)]
    unnamed x12 -> x0, other arithmetic: 3.86 us -> none
  transfers between devices with their start and end apart: 2 -> 0, of which waited for: 2 -> 0; matrix products, arithmetic and copies ran while one was open for 9% -> 0% of each run, Pallas kernels for 0% -> 0%
where the time goes in v2:
time: 91.5 us; the launch traced here: 91.4 us
  Pallas kernels  89.1 us (97%)
  local copies, waits for them, and re-layouts  2.26 us (2%)
    pallas_call x1, Pallas kernels, on_device_fused(): pl.pallas_call(functools.partial(fused_kernel, (row_count, col_count)), o...  89.1 us
    unnamed x1, local copies, waits for them, and re-layouts  2.26 us

profile of v2, /device:TPU:17, one launch (start us, length us, event | category | flops | bytes accessed | tf_op | source)
XLA Modules:
  0.0 91.4 jit_solution(10913771951963659854)
XLA Ops:
  0.0 89.1 %shard_map.64 = bf16[512,1024]{1,0:T(8,128)(2,1)} custom-call(bf16[512,1024]{1,0:T(8,128)(2,1)} %x_ref.1, f32[1,4096]{1,0:T(1,128)} %bitcast.1, bf16[1024,1024]{1,0:T(8,128)(2,1)} %constant.6.clone.table_ref, bf16[512,1024]{1,0:T(8,128)(2,1)} %constant.7.clone.low_ref, f32[512,128]{1,0:T(8,128)} %constant.8.clone.twist_ref, bf16[4096,1024]{1,0:T(8,128)(2,1)} %w_hbm.1), custom_call_target="tpu_custom_call" | custom-call | tf_op jit(solution)/shard_map/pallas_call | solution.py:421
  89.1 2.3 %copy.8 = bf16[512,1024]{1,0:T(8,128)(2,1)} copy(bf16[512,1024]{1,0:T(8,128)(2,1)} %shard_map.64) | data formatting | bytes 2097152

commit v3 on v2

--- a/solution.py
+++ b/solution.py
@@ -129,8 +129,8 @@
 
 
 def fused_kernel(
-    dims, x_ref, gain_ref, table_ref, low_ref, twist_ref, w_hbm, out_ref,
-    w_ref, fold_ref, folded, send1, recv1, sums, stacked, send2, lhs, acc, spread,
+    dims, x_ref, gain_ref, table_hbm, low_hbm, twist_hbm, w_hbm, out_ref,
+    table_ref, low_ref, twist_ref, w_ref, fold_ref, folded, send1, recv1, sums, stacked, send2, lhs, acc, spread,
     w_sem, s_send, s_recv, a_send, a_recv, b_send, b_recv, g_send, g_recv, l_sem,
 ):
     row_count, col_count = dims
@@ -150,8 +150,12 @@
     y_next = 2 * (1 - c // 2) + c % 2
     diagonal = 2 * (1 - c // 2) + 1 - c % 2
     col_peers = (x_next, y_next, diagonal)
+    table_copy = pltpu.make_async_copy(table_hbm, table_ref, l_sem.at[2])
     w_copy = pltpu.make_async_copy(w_hbm, w_ref, w_sem)
-    w_copy.start()
+    low_copy = pltpu.make_async_copy(low_hbm, low_ref, l_sem.at[3])
+    twist_copy = pltpu.make_async_copy(twist_hbm, twist_ref, l_sem.at[4])
+    for copy in (table_copy, w_copy, low_copy, twist_copy):
+        copy.start()
 
     barrier = pltpu.get_barrier_semaphore()
     for step in range(1, row_count):
@@ -185,6 +189,7 @@
     far_first = sorted(range(chips), key=lambda d: -min(d, chips - d))
     first_copies = []
     inv = None
+    table_copy.wait()
     for d in far_first:
         chip = lax.rem(z + d, chips)
         product = jnp.dot(
@@ -257,6 +262,8 @@
         return 2 * lax.rem(z - d + chips, chips) + i
 
     stay1.wait()
+    twist_copy.wait()
+    low_copy.wait()
     arrived(recv1.at[other], a_recv.at[0])
     for d in range(1, chips):
         for i in range(2):
@@ -304,8 +311,31 @@
     def lanes_of(index):
         return pl.ds(pl.multiple_of(index * slab, slab), slab)
 
-    second_copies = {}
-    for d in far_first:
+    sends = []
+
+    def share(origin, source, block, target, out_slot, in_slot):
+        copy = pltpu.make_async_remote_copy(
+            src_ref=source, dst_ref=lhs.at[origin, :, :, lanes_of(block)],
+            send_sem=g_send.at[out_slot], recv_sem=g_recv.at[in_slot],
+            device_id=(r, target), device_id_type=MESH,
+        )
+        copy.start()
+        sends.append(copy)
+        return copy
+
+    def held(origin, block):
+        return lhs.at[origin, :, :, lanes_of(block)]
+
+    count = row_count
+    from_x, from_y, from_far = [], [], []
+
+    def offer(n, source, block):
+        from_x.append(share(c, source, block, x_next, n, n))
+        from_y.append(share(c, source, block, y_next, count + n, count + n))
+
+    second_copies = []
+    stay2 = pltpu.make_async_copy(send2.at[r], held(c, r), l_sem.at[1])
+    for d in [0] + far_first[:-1]:
         chip = lax.rem(z + d, chips)
         lows = jnp.dot(
             low_ref[pl.ds(pl.multiple_of(chip * 2 * part, 2 * part), 2 * part), :], stacked[...],
@@ -316,63 +346,31 @@
                 send2[2 * chip + i, q] = lows[i * part : (i + 1) * part, q * slab : (q + 1) * slab]
         for target, slot in ([(2 * chip, 2 * d), (2 * chip + 1, 2 * d + 1)] if d else [(other, 0)]):
             copy = pltpu.make_async_remote_copy(
-                src_ref=send2.at[target], dst_ref=lhs.at[c, :, :, lanes_of(r)],
+                src_ref=send2.at[target], dst_ref=held(c, r),
                 send_sem=b_send.at[slot],
                 recv_sem=b_recv.at[slot] if d == 0 else b_recv.at[2 * d + r % 2],
                 device_id=(target, c), device_id_type=MESH,
             )
             copy.start()
-            second_copies[slot] = copy
-    stay2 = pltpu.make_async_copy(send2.at[r], lhs.at[c, :, :, lanes_of(r)], l_sem.at[1])
-    stay2.start()
-
-    sends = []
-
-    def share(origin, source, block, target, out_slot, in_slot):
-        copy = pltpu.make_async_remote_copy(
-            src_ref=source, dst_ref=lhs.at[origin, :, :, lanes_of(block)],
-            send_sem=g_send.at[out_slot], recv_sem=g_recv.at[in_slot],
-            device_id=(r, target), device_id_type=MESH,
-        )
-        copy.start()
-        sends.append(copy)
-        return copy
-
-    def held(origin, block):
-        return lhs.at[origin, :, :, lanes_of(block)]
-
-    order = [(None, r), (None, other)]
-    for d in sorted(range(1, chips), key=lambda d: min(d, chips - d)):
-        order += [((2 * d + i), block_of(d, i)) for i in range(2)]
-    count = len(order)
-    from_x, from_y, from_far = [], [], []
-    for n in range(count + 1):
-        if n < count:
-            slot, block = order[n]
-            if n == 0:
-                stay2.wait()
-            else:
-                arrived(held(c, block), b_recv.at[0 if n == 1 else slot])
-            source = held(c, block)
-            from_x.append(share(c, source, block, x_next, n, n))
-            from_y.append(share(c, source, block, y_next, count + n, count + n))
-        if n:
-            _, block = order[n - 1]
-            slot = 2 * count + n - 1
-            if n % 2:
-                from_x[n - 1].wait_recv()
-                from_far.append(share(x_next, held(x_next, block), block, y_next, slot, slot))
-            else:
-                from_y[n - 1].wait_recv()
-                from_far.append(share(y_next, held(y_next, block), block, x_next, slot, slot))
-
-    def multiply(origin, first, last):
-        base = pl.multiple_of(origin * group_len, group_len)
+            second_copies.append(copy)
+        if d == 0:
+            offer(0, send2.at[r], r)
+            stay2.start()
+
+    near_first = sorted(range(chips), key=lambda d: min(d, chips - d))
+    pairs = [lax.rem(z - d + chips, chips) for d in near_first]
+    order = [(None, r), (0, other)]
+    for d in near_first[1:]:
+        order += [(2 * d + i, block_of(d, i)) for i in range(2)]
+
+    def multiply(origin, m, first=False, last=False):
+        base = pl.multiple_of(origin * group_len + pairs[m] * pair, pair)
+        taken = pl.ds(pl.multiple_of(pairs[m] * pair, pair), pair)
 
         def step(i, carry):
             cols = pl.ds(pl.multiple_of(i * wide, wide), wide)
-            left = lhs[origin].reshape(block_len, group_len)
-            value = jnp.dot(left, folded[pl.ds(base, group_len), cols], preferred_element_type=F32)
+            left = lhs[origin, :, :, taken].reshape(block_len, pair)
+            value = jnp.dot(left, folded[pl.ds(base, pair), cols], preferred_element_type=F32)
             if not first:
                 value = acc[:, cols] + value
             if not last:
@@ -390,18 +388,55 @@
 
         lax.fori_loop(0, pieces, step, 0)
 
-    multiply(c, True, False)
-    for n in range(1, count, 2):
-        from_x[n].wait_recv()
-    multiply(x_next, False, False)
-    for n in range(0, count, 2):
-        from_y[n].wait_recv()
-    multiply(y_next, False, False)
-    for copy in from_far:
-        copy.wait_recv()
-    multiply(diagonal, False, True)
-
-    for copy in sum_copies + first_copies + list(second_copies.values()) + sends:
+    def own_part(m):
+        if m == 0:
+            stay2.wait()
+        multiply(c, m, first=m == 0)
+
+    def x_part(m):
+        from_x[2 * m + 1].wait_recv()
+        multiply(x_next, m)
+
+    def y_part(m):
+        from_y[2 * m].wait_recv()
+        multiply(y_next, m)
+
+    def far_part(m):
+        from_far[2 * m].wait_recv()
+        from_far[2 * m + 1].wait_recv()
+        multiply(diagonal, m, last=m == chips - 1)
+
+    for n in range(1, count + 1):
+        if n < count:
+            slot, block = order[n]
+            arrived(held(c, block), b_recv.at[slot])
+            offer(n, held(c, block), block)
+        _, block = order[n - 1]
+        slot = 2 * count + n - 1
+        if n % 2:
+            from_x[n - 1].wait_recv()
+            from_far.append(share(x_next, held(x_next, block), block, y_next, slot, slot))
+        else:
+            from_y[n - 1].wait_recv()
+            from_far.append(share(y_next, held(y_next, block), block, x_next, slot, slot))
+        m = n // 2
+        if n % 2:
+            own_part(m)
+            if m:
+                x_part(m - 1)
+        elif 2 <= m < chips:
+            y_part(m - 2)
+            if m >= 3:
+                far_part(m - 3)
+    y_part(chips - 2)
+    for m in range(max(chips - 3, 0), chips - 2):
+        far_part(m)
+    x_part(chips - 1)
+    y_part(chips - 1)
+    far_part(chips - 2)
+    far_part(chips - 1)
+
+    for copy in sum_copies + first_copies + second_copies + sends:
         copy.wait_send()
 
 
@@ -421,9 +456,12 @@
     return pl.pallas_call(
         functools.partial(fused_kernel, (row_count, col_count)),
         out_shape=jax.ShapeDtypeStruct((block_len, out_width), BF16),
-        in_specs=[vmem] * 5 + [pl.BlockSpec(memory_space=pl.ANY)],
+        in_specs=[vmem] * 2 + [pl.BlockSpec(memory_space=pl.ANY)] * 4,
         out_specs=vmem,
         scratch_shapes=[
+            pltpu.VMEM(chan_table.shape, BF16),
+            pltpu.VMEM(low_table.shape, BF16),
+            pltpu.VMEM(twist.shape, F32),
             pltpu.VMEM(out_weight.shape, BF16),
             pltpu.VMEM((row_count // 2, 2 * slab, 4 * slab), BF16),
             pltpu.VMEM(out_weight.shape, BF16),
@@ -437,7 +475,7 @@
             pltpu.VMEM((2, block_len, 128), F32),
             dma, dma((col_count - 1,)), dma((col_count - 1,)),
             dma((row_count,)), dma((row_count,)), dma((row_count,)), dma((row_count,)),
-            dma((3 * row_count,)), dma((3 * row_count,)), dma((2,)),
+            dma((3 * row_count,)), dma((3 * row_count,)), dma((5,)),
         ],
         compiler_params=pltpu.CompilerParams(
             collective_id=0, has_side_effects=True, vmem_limit_bytes=60 * 1024 * 1024

time: 91.5 us -> 88.3 us (0.965)
  Pallas kernels: 89.1 us -> 85.9 us
    pallas_call x1, Pallas kernels: 89.1 us -> 85.9 us  [on_device_fused(): pl.pallas_call(functools.partial(fused_kernel, (row_count, col_count)), o...]
where the time goes in v3:
time: 88.3 us; the launch traced here: 88.2 us
  Pallas kernels  85.9 us (97%)
  local copies, waits for them, and re-layouts  2.26 us (3%)
    pallas_call x1, Pallas kernels, on_device_fused(): pl.pallas_call(functools.partial(fused_kernel, (row_count, col_count)), o...  85.9 us
    unnamed x1, local copies, waits for them, and re-layouts  2.26 us

profile of v3, /device:TPU:17, one launch (start us, length us, event | category | flops | bytes accessed | tf_op | source)
XLA Modules:
  0.0 88.2 jit_solution(1269416314928724111)
XLA Ops:
  0.0 85.9 %shard_map.64 = bf16[512,1024]{1,0:T(8,128)(2,1)} custom-call(bf16[512,1024]{1,0:T(8,128)(2,1)} %x_ref.1, f32[1,4096]{1,0:T(1,128)} %bitcast.1, bf16[1024,1024]{1,0:T(8,128)(2,1)} %constant.6.clone.table_hbm, bf16[512,1024]{1,0:T(8,128)(2,1)} %constant.7.clone.low_hbm, f32[512,128]{1,0:T(8,128)} %constant.8.clone.twist_hbm, bf16[4096,1024]{1,0:T(8,128)(2,1)} %w_hbm.1), custom_call_target="tpu_custom_call" | custom-call | tf_op jit(solution)/shard_map/pallas_call | solution.py:456
  85.9 2.3 %copy.8 = bf16[512,1024]{1,0:T(8,128)(2,1)} copy(bf16[512,1024]{1,0:T(8,128)(2,1)} %shard_map.64) | data formatting | bytes 2097152

commit v4 on v3

--- a/solution.py
+++ b/solution.py
@@ -130,7 +130,7 @@
 
 def fused_kernel(
     dims, x_ref, gain_ref, table_hbm, low_hbm, twist_hbm, w_hbm, out_ref,
-    table_ref, low_ref, twist_ref, w_ref, fold_ref, folded, send1, recv1, sums, stacked, send2, lhs, acc, spread,
+    table_ref, low_ref, twist_in, twist_ref, w_ref, fold_ref, folded, send1, recv1, sums, stacked, send2, lhs, acc,
     w_sem, s_send, s_recv, a_send, a_recv, b_send, b_recv, g_send, g_recv, l_sem,
 ):
     row_count, col_count = dims
@@ -141,7 +141,7 @@
     pair = 2 * slab
     chips = row_count // 2
     part = block_len // row_count
-    out_width = out_ref.shape[1]
+    out_width = out_ref.shape[2]
     r = lax.axis_index("row")
     c = lax.axis_index("col")
     z = r // 2
@@ -153,7 +153,7 @@
     table_copy = pltpu.make_async_copy(table_hbm, table_ref, l_sem.at[2])
     w_copy = pltpu.make_async_copy(w_hbm, w_ref, w_sem)
     low_copy = pltpu.make_async_copy(low_hbm, low_ref, l_sem.at[3])
-    twist_copy = pltpu.make_async_copy(twist_hbm, twist_ref, l_sem.at[4])
+    twist_copy = pltpu.make_async_copy(twist_hbm, twist_in, l_sem.at[4])
     for copy in (table_copy, w_copy, low_copy, twist_copy):
         copy.start()
 
@@ -164,8 +164,6 @@
         )
     for peer in col_peers:
         pl.semaphore_signal(barrier, inc=1, device_id=(r, peer), device_id_type=MESH)
-    pl.semaphore_wait(barrier, row_count + col_count - 2)
-
     values = x_ref[...].astype(F32)
     squares = values * values
     top = squares.astype(BF16)
@@ -175,6 +173,7 @@
     own = lax.dot_general(ones, top, lanes, preferred_element_type=F32)
     own = own + lax.dot_general(ones, rest, lanes, preferred_element_type=F32)
     sums[c] = own[:8]
+    pl.semaphore_wait(barrier, row_count + col_count - 2)
     sum_copies = []
     for k, peer in enumerate(col_peers):
         copy = pltpu.make_async_remote_copy(
@@ -232,6 +231,9 @@
         signed = jnp.where(odd, -1.0, 1.0)
         fold_ref[t] = jnp.where(direct, signed, jnp.where(mirror | middle, 1.0, 0.0)).astype(BF16)
 
+    twist_copy.wait()
+    filler = jnp.zeros((128 - 2 * row_count, block_len), F32)
+    twist_ref[...] = jnp.transpose(jnp.concatenate([twist_in[...], filler], 0))
     w_copy.wait()
     wide = 256
     pieces = out_width // wide
@@ -262,7 +264,6 @@
         return 2 * lax.rem(z - d + chips, chips) + i
 
     stay1.wait()
-    twist_copy.wait()
     low_copy.wait()
     arrived(recv1.at[other], a_recv.at[0])
     for d in range(1, chips):
@@ -376,14 +377,7 @@
             if not last:
                 acc[:, cols] = value
             else:
-                for q in range(row_count):
-                    for j in range(wide // 128):
-                        spread[j, pl.ds(q, part, stride=row_count), :] = value[
-                            q * part : (q + 1) * part, j * 128 : (j + 1) * 128
-                        ]
-                for j in range(wide // 128):
-                    at = pl.ds(pl.multiple_of(i * wide + j * 128, 128), 128)
-                    out_ref[:, at] = spread[j].astype(BF16)
+                out_ref[:, :, cols] = value.astype(BF16).reshape(row_count, part, wide)
             return carry
 
         lax.fori_loop(0, pieces, step, 0)
@@ -448,20 +442,19 @@
     slab = group_len // row_count
     part = block_len // row_count
     chan_table, low_table, twist_cos, twist_sin = host_tables(group_len, row_count, block_len)
-    twist = np.zeros((block_len, 128), np.float32)
-    twist[:, :row_count] = twist_cos.T
-    twist[:, row_count : 2 * row_count] = twist_sin.T
+    twist = np.concatenate([twist_cos, twist_sin], 0).astype(np.float32)
     vmem = pl.BlockSpec(memory_space=pltpu.VMEM)
     dma = pltpu.SemaphoreType.DMA
-    return pl.pallas_call(
+    mapped = pl.pallas_call(
         functools.partial(fused_kernel, (row_count, col_count)),
-        out_shape=jax.ShapeDtypeStruct((block_len, out_width), BF16),
+        out_shape=jax.ShapeDtypeStruct((row_count, part, out_width), BF16),
         in_specs=[vmem] * 2 + [pl.BlockSpec(memory_space=pl.ANY)] * 4,
         out_specs=vmem,
         scratch_shapes=[
             pltpu.VMEM(chan_table.shape, BF16),
             pltpu.VMEM(low_table.shape, BF16),
             pltpu.VMEM(twist.shape, F32),
+            pltpu.VMEM((block_len, 128), F32),
             pltpu.VMEM(out_weight.shape, BF16),
             pltpu.VMEM((row_count // 2, 2 * slab, 4 * slab), BF16),
             pltpu.VMEM(out_weight.shape, BF16),
@@ -472,7 +465,6 @@
             pltpu.VMEM((row_count, row_count, part, slab), BF16),
             pltpu.VMEM((col_count, row_count, part, group_len), BF16),
             pltpu.VMEM((block_len, out_width), F32),
-            pltpu.VMEM((2, block_len, 128), F32),
             dma, dma((col_count - 1,)), dma((col_count - 1,)),
             dma((row_count,)), dma((row_count,)), dma((row_count,)), dma((row_count,)),
             dma((3 * row_count,)), dma((3 * row_count,)), dma((5,)),
@@ -484,6 +476,7 @@
         tokens, norm_gain[None, :], jnp.asarray(chan_table, BF16), jnp.asarray(low_table, BF16),
         jnp.asarray(twist), out_weight,
     )
+    return jnp.transpose(mapped, (1, 0, 2)).reshape(block_len, out_width)
 
 
 def on_device(tokens, norm_gain, out_weight):

time: 88.3 us -> 87.8 us (level)
  Pallas kernels: 85.9 us -> 84.8 us
    transpose x0 -> x1, local copies, waits for them, and re-layouts: none -> 2.77 us  [on_device_fused(): return jnp.transpose(mapped, (1, 0, 2)).reshape(block_len, out_width)]
    unnamed x1 -> x0, local copies, waits for them, and re-layouts: 2.26 us -> none
    pallas_call x1, Pallas kernels: 85.9 us -> 84.8 us  [on_device_fused(): pl.pallas_call(functools.partial(fused_kernel, (row_count, col_count)), o...]
where the time goes in v4:
time: 87.8 us; the launch traced here: 87.6 us
  Pallas kernels  84.8 us (97%)
  local copies, waits for them, and re-layouts  2.77 us (3%)
    pallas_call x1, Pallas kernels, on_device_fused(): pl.pallas_call(functools.partial(fused_kernel, (row_count, col_count)), o...  84.8 us
    transpose x1, local copies, waits for them, and re-layouts, on_device_fused(): return jnp.transpose(mapped, (1, 0, 2)).reshape(block_len, out_width)  2.77 us

profile of v4, /device:TPU:17, one launch (start us, length us, event | category | flops | bytes accessed | tf_op | source)
XLA Modules:
  0.0 87.6 jit_solution(7905273535620057424)
XLA Ops:
  0.0 84.8 %shard_map.64 = bf16[8,64,1024]{2,1,0:T(8,128)(2,1)} custom-call(bf16[512,1024]{1,0:T(8,128)(2,1)} %x_ref.1, f32[1,4096]{1,0:T(1,128)} %bitcast.6, bf16[1024,1024]{1,0:T(8,128)(2,1)} %constant.6.clone.table_hbm, bf16[512,1024]{1,0:T(8,128)(2,1)} %constant.7.clone.low_hbm, f32[16,512]{1,0:T(8,128)} %constant.8.clone.twist_hbm, bf16[4096,1024]{1,0:T(8,128)(2,1)} %w_hbm.1), custom_call_target="tpu_custom_call" | custom-call | tf_op jit(solution)/shard_map/pallas_call | solution.py:448
  84.8 2.8 %copy.9 = bf16[64,8,1024]{2,1,0:T(8,128)(2,1)} copy(bf16[64,8,1024]{2,0,1:T(8,128)(2,1)} %bitcast.5) | data formatting | bytes 2097152 | tf_op jit(solution)/shard_map/transpose | solution.py:479

commit v5 on v4

--- a/solution.py
+++ b/solution.py
@@ -336,7 +336,8 @@
 
     second_copies = []
     stay2 = pltpu.make_async_copy(send2.at[r], held(c, r), l_sem.at[1])
-    for d in [0] + far_first[:-1]:
+    near_first = sorted(range(chips), key=lambda d: min(d, chips - d))
+    for d in near_first:
         chip = lax.rem(z + d, chips)
         lows = jnp.dot(
             low_ref[pl.ds(pl.multiple_of(chip * 2 * part, 2 * part), 2 * part), :], stacked[...],
@@ -358,7 +359,6 @@
             offer(0, send2.at[r], r)
             stay2.start()
 
-    near_first = sorted(range(chips), key=lambda d: min(d, chips - d))
     pairs = [lax.rem(z - d + chips, chips) for d in near_first]
     order = [(None, r), (0, other)]
     for d in near_first[1:]:

time: 87.8 us -> 85.4 us (0.973)
  Pallas kernels: 84.8 us -> 82.2 us
    pallas_call x1, Pallas kernels: 84.8 us -> 82.2 us  [on_device_fused(): pl.pallas_call(functools.partial(fused_kernel, (row_count, col_count)), o...]
where the time goes in v5:
time: 85.4 us; the launch traced here: 85 us
  Pallas kernels  82.2 us (96%)
  local copies, waits for them, and re-layouts  2.77 us (3%)
    pallas_call x1, Pallas kernels, on_device_fused(): pl.pallas_call(functools.partial(fused_kernel, (row_count, col_count)), o...  82.2 us
    transpose x1, local copies, waits for them, and re-layouts, on_device_fused(): return jnp.transpose(mapped, (1, 0, 2)).reshape(block_len, out_width)  2.77 us

profile of v5, /device:TPU:17, one launch (start us, length us, event | category | flops | bytes accessed | tf_op | source)
XLA Modules:
  0.0 85.0 jit_solution(4580366569070548923)
XLA Ops:
  0.0 82.2 %shard_map.64 = bf16[8,64,1024]{2,1,0:T(8,128)(2,1)} custom-call(bf16[512,1024]{1,0:T(8,128)(2,1)} %x_ref.1, f32[1,4096]{1,0:T(1,128)} %bitcast.6, bf16[1024,1024]{1,0:T(8,128)(2,1)} %constant.6.clone.table_hbm, bf16[512,1024]{1,0:T(8,128)(2,1)} %constant.7.clone.low_hbm, f32[16,512]{1,0:T(8,128)} %constant.8.clone.twist_hbm, bf16[4096,1024]{1,0:T(8,128)(2,1)} %w_hbm.1), custom_call_target="tpu_custom_call" | custom-call | tf_op jit(solution)/shard_map/pallas_call | solution.py:448
  82.2 2.8 %copy.9 = bf16[64,8,1024]{2,1,0:T(8,128)(2,1)} copy(bf16[64,8,1024]{2,0,1:T(8,128)(2,1)} %bitcast.5) | data formatting | bytes 2097152 | tf_op jit(solution)/shard_map/transpose | solution.py:479
